TPU v7x, 32 devices: a whole 2x2x4 slice. The times are simulated.
32 devices in a mesh: grp: 1, ep: 32 (over z, y, x, core).
Axes of the slice: x: 2, y: 2, z: 4, core: 2. Of those that a mesh axis runs over, the one named last changes fastest.
Arguments:
- tokens: bfloat16 [64, 2048], P('grp', 'ep'), may hold values from -6 to 6
- w_query: bfloat16 [2048, 1024], P('ep'), may hold values from -0.125 to 0.125
- w_key: bfloat16 [2048, 1024], P('ep'), may hold values from -0.125 to 0.125
- w_value: bfloat16 [2048, 1024], P('ep'), may hold values from -0.125 to 0.125
- w_forget: bfloat16 [2048, 16], P('ep'), may hold values from -0.125 to 0.125
- forget_bias: float32 [16], replicated, may hold values from -1 to 2
- cache_keys: bfloat16 [64, 1024, 1024], P(('grp', 'ep'))
- cache_values: bfloat16 [64, 1024, 1024], P(('grp', 'ep')), may hold values from -6 to 6
- cache_gates: float32 [64, 1024, 16], P(('grp', 'ep')), as said below
- lengths: int32 [64], P(('grp', 'ep')), may hold values from 128 to 1024, as said below
- w_out: bfloat16 [1024, 2048], P('ep'), may hold values from -0.1875 to 0.1875
- norm_gain: bfloat16 [2048], replicated, may hold values from 0.099609375 to 1.8984375
- w_router: bfloat16 [2048, 4], replicated, may hold values from -0.125 to 0.125
- routes: int32 [64, 2], P('grp'), may hold values from 0 to 3, all different within a row
- dense_gate: bfloat16 [2048], replicated, may hold values from -0.25 to 0.25
- dense_w_gate: bfloat16 [2048, 8192], P(None, 'ep'), may hold values from -0.125 to 0.125
- dense_w_up: bfloat16 [2048, 8192], P(None, 'ep'), may hold values from -0.125 to 0.125
- dense_w_down: bfloat16 [8192, 2048], P('ep'), may hold values from -0.125 to 0.125
- expert_w_gate: bfloat16 [2048, 16384], P(None, 'ep'), may hold values from -0.125 to 0.125
- expert_w_up: bfloat16 [2048, 16384], P(None, 'ep'), may hold values from -0.125 to 0.125
- expert_w_down: bfloat16 [16384, 2048], P('ep'), may hold values from -0.1875 to 0.1875
- final_gain: bfloat16 [2048], P('ep'), may hold values from 0.099609375 to 1.8984375
Outputs:
- result: bfloat16 [64, 2048], P('grp', 'ep')
Inputs may be any that keep to these rules, and one draw needn't show every extreme that they name: `routes`: each row names 2 different experts; every expert is named by some row. `lengths`: the first sequence of each part holds 1024 positions. `cache_gates`: never rising along positions.
All inputs are finite; a program needn't handle non-finite values.
Results may differ from a plain program's by a relative error of at most 0.0085.
Values may be sent and summed in bfloat16 or wider, within the bound.
A program may use at most 128 MiB of HBM per device.

v0:
```python
import jax
import jax.numpy as jnp
from jax import lax
from jax.sharding import PartitionSpec as P

EXP_SPLIT = 8
norm_eps = 1e-05
residual_scale = 8.0**0.25


def norm_rows(values, weights):
    center = jnp.mean(values, axis=-1, keepdims=True)
    second = jnp.mean(values * values, axis=-1, keepdims=True)
    return (
        (values - center)
        * lax.rsqrt(second - center * center + norm_eps)
        * weights.astype(jnp.float32)
    )


def attend(
    query,
    new_key,
    new_value,
    forget_pre,
    forget_bias,
    cache_keys,
    cache_values,
    cache_gates,
    lengths,
):
    seqs_here, width = query.shape
    heads = cache_gates.shape[2]
    head_size = width // heads
    cache_len = cache_keys.shape[1]
    query = query.reshape(seqs_here, heads, head_size)
    new_key = new_key.reshape(seqs_here, heads, head_size)
    new_value = new_value.reshape(seqs_here, heads, head_size)
    keys_all = cache_keys.reshape(seqs_here, cache_len, heads, head_size)
    values_all = cache_values.reshape(seqs_here, cache_len, heads, head_size)
    log_gate = jax.nn.log_sigmoid(forget_pre + forget_bias[None, :])
    position = jnp.arange(cache_len, dtype=jnp.int32)
    is_last = (position[None, :] == (lengths - 1)[:, None]).astype(jnp.float32)
    last_gate = jnp.sum(cache_gates * is_last[:, :, None], axis=1)
    bias = (last_gate + log_gate)[:, :, None] - jnp.transpose(cache_gates, (0, 2, 1))
    scale = head_size ** (-0.5)
    scores = (
        jnp.einsum("shd,slhd->shl", query, keys_all, preferred_element_type=jnp.float32) * scale
        + bias
    )
    valid = (position[None, :] < lengths[:, None])[:, None, :]
    scores = jnp.where(valid, scores, -jnp.inf)
    own_score = jnp.sum(query.astype(jnp.float32) * new_key.astype(jnp.float32), axis=-1) * scale
    top = jnp.maximum(jnp.max(scores, axis=-1), own_score)
    weights_cache = jnp.exp(scores - top[:, :, None])
    weight_own = jnp.exp(own_score - top)
    total = jnp.sum(weights_cache, axis=-1) + weight_own
    probs = (weights_cache / total[:, :, None]).astype(jnp.bfloat16)
    prob_own = (weight_own / total).astype(jnp.bfloat16)
    mixed = jnp.einsum("shl,slhd->shd", probs, values_all, preferred_element_type=jnp.float32)
    mixed = mixed + prob_own.astype(jnp.float32)[:, :, None] * new_value.astype(jnp.float32)
    return mixed.astype(jnp.bfloat16).reshape(seqs_here, width)


def shards(
    tokens,
    w_query,
    w_key,
    w_value,
    w_forget,
    forget_bias,
    cache_keys,
    cache_values,
    cache_gates,
    lengths,
    w_out,
    norm_gain,
    w_router,
    routes,
    dense_gate,
    dense_w_gate,
    dense_w_up,
    dense_w_down,
    expert_w_gate,
    expert_w_up,
    expert_w_down,
    final_gain,
):
    rank = lax.axis_index("ep")
    seqs_all, feat_dev = tokens.shape
    offset = rank * feat_dev
    terms = (
        jnp.dot(tokens, w_query, preferred_element_type=jnp.float32),
        jnp.dot(tokens, w_key, preferred_element_type=jnp.float32),
        jnp.dot(tokens, w_value, preferred_element_type=jnp.float32),
        jnp.dot(tokens, w_forget, preferred_element_type=jnp.float32),
    )
    query_sum, key_sum, value_sum, forget_pre = (
        lax.psum_scatter(terms[0], "ep", scatter_dimension=0, tiled=True),
        lax.psum_scatter(terms[1], "ep", scatter_dimension=0, tiled=True),
        lax.psum_scatter(terms[2], "ep", scatter_dimension=0, tiled=True),
        lax.psum_scatter(terms[3], "ep", scatter_dimension=0, tiled=True),
    )
    attn = attend(
        query_sum.astype(jnp.bfloat16),
        key_sum.astype(jnp.bfloat16),
        value_sum.astype(jnp.bfloat16),
        forget_pre,
        forget_bias,
        cache_keys,
        cache_values,
        cache_gates,
        lengths,
    )
    head_cols = lax.all_to_all(attn, "ep", split_axis=1, concat_axis=0, tiled=True)
    partial_sum = jnp.dot(head_cols, w_out, preferred_element_type=jnp.float32)
    residual = residual_scale * tokens.astype(jnp.float32)
    placed = lax.dynamic_slice_in_dim(partial_sum, offset, feat_dev, 1) + residual
    mixed = lax.psum(lax.dynamic_update_slice_in_dim(partial_sum, placed, offset, 1), "ep")
    normed = norm_rows(mixed, norm_gain).astype(jnp.bfloat16)
    logits = jnp.dot(normed, w_router, preferred_element_type=jnp.float32)
    expert_count = w_router.shape[1]
    picks = (routes[:, :, None] == jnp.arange(expert_count, dtype=jnp.int32)[None, None, :]).astype(
        jnp.float32
    )
    chosen = jnp.sum(logits[:, None, :] * picks, axis=-1)
    route_weight = jax.nn.softmax(chosen, axis=-1)
    expert_id = rank // EXP_SPLIT
    mine = jnp.sum(route_weight * (routes == expert_id).astype(jnp.float32), axis=1)
    expert_gate_part = jnp.dot(normed, expert_w_gate, preferred_element_type=jnp.float32)
    expert_up_part = jnp.dot(normed, expert_w_up, preferred_element_type=jnp.float32)
    expert_hidden = (mine[:, None] * jax.nn.silu(expert_gate_part) * expert_up_part).astype(
        jnp.bfloat16
    )
    dense_scale = jax.nn.sigmoid(jnp.dot(normed, dense_gate, preferred_element_type=jnp.float32))
    dense_gate_part = jnp.dot(normed, dense_w_gate, preferred_element_type=jnp.float32)
    dense_up_part = jnp.dot(normed, dense_w_up, preferred_element_type=jnp.float32)
    dense_hidden = (dense_scale[:, None] * jax.nn.silu(dense_gate_part) * dense_up_part).astype(
        jnp.bfloat16
    )
    local_branch = jnp.dot(
        expert_hidden, expert_w_down, preferred_element_type=jnp.float32
    ) + jnp.dot(dense_hidden, dense_w_down, preferred_element_type=jnp.float32)
    branch = lax.psum(local_branch, "ep")
    final = residual_scale * normed.astype(jnp.float32) + branch
    center = jnp.mean(final, axis=-1, keepdims=True)
    second = jnp.mean(final * final, axis=-1, keepdims=True)
    unit = (final - center) * lax.rsqrt(second - center * center + norm_eps)
    result = (
        lax.dynamic_slice_in_dim(unit, offset, feat_dev, 1)
        * final_gain.astype(jnp.float32)[None, :]
    )
    return result.astype(jnp.bfloat16)


def solution(mesh):
    placed = (
        P("grp", "ep"),
        P("ep", None),
        P("ep", None),
        P("ep", None),
        P("ep", None),
        P(),
        P(("grp", "ep"), None, None),
        P(("grp", "ep"), None, None),
        P(("grp", "ep"), None, None),
        P(("grp", "ep")),
        P("ep", None),
        P(),
        P(),
        P("grp", None),
        P(),
        P(None, "ep"),
        P(None, "ep"),
        P("ep", None),
        P(None, "ep"),
        P(None, "ep"),
        P("ep", None),
        P("ep"),
    )
    return jax.shard_map(
        shards, mesh=mesh, in_specs=placed, out_specs=P("grp", "ep"), check_vma=False
    )
```

profile of v0, /device:TPU:0, one launch (start us, length us, event | category | flops | bytes accessed | tf_op | source)
XLA Modules:
  0.0 374.7 jit_solution(17475962631380918628)
XLA Ops:
  6.5 0.0 copy-start
  6.5 0.8 broadcast_add_fusion
  7.3 0.7 iota_compare_fusion
  8.1 0.8 fusion.49
  8.9 1.1 fusion.47
  10.0 1.1 fusion.50
  11.1 1.1 fusion.51
  12.2 52.3 %all-reduce.12 = (bf16[64,1024]{1,0:T(8,128)(2,1)S(1)}, f32[64,16]{1,0:T(8,128)S(1)}, bf16[64,1024]{1,0:T(8,128)(2,1)S(1)}, bf16[64,1024]{1,0:T(8,128)(2,1)S(1)}) all-reduce(f32[64,1024]{1,0:T(8,128)S(1)} %fusion.47, f32[64,16]{1,0:T(8,128)S(1)} %fusion.49, f32[64,1024]{1,0:T(8,128)S(1)} %fusion.50, ...), channel_id=2, replica_groups=mesh['grp'=1,'ep'=32] {'ep'}, use_global_device_ids=true, to_apply=%region_0.0.clone | all-reduce | flops 197632 | bytes 1187840
  64.5 0.1 reshape.129
  64.6 0.1 reshape.141
  64.7 0.1 compare_convert_fusion
  64.8 0.1 reshape.133
  64.9 0.1 reshape.132
  65.0 0.0 copy-start.3
  65.0 6.2 %copy.39 = bf16[2,1024,1024]{1,2,0:T(8,128)(2,1)} copy(bf16[2,1024,1024]{2,1,0:T(8,128)(2,1)} %param.28) | data formatting | bytes 8388608 | tf_op args[6]
  71.2 0.0 copy-done.3
  71.2 0.1 multiply_reduce_fusion.2
  71.3 0.1 multiply_reduce_fusion.3
  71.4 0.0 copy-start.10
  71.4 2.9 fusion.48
  74.3 0.0 copy-done.10
  74.3 0.2 fusion.45
  74.5 0.2 fusion.16
  74.7 0.1 fusion.25
  74.8 6.2 %copy.40 = bf16[2,1024,1024]{1,2,0:T(8,128)(2,1)} copy(bf16[2,1024,1024]{2,1,0:T(8,128)(2,1)} %param.29) | data formatting | bytes 8388608 | tf_op args[7]
  81.0 0.0 copy-start.4
  81.0 3.4 fusion.8
  84.4 0.1 add_convert_fusion
  84.5 0.1 all_to_all.14
  84.6 0.6 copy.41
  85.2 3.4 all-to-all-start
  88.6 0.0 all-reduce.9.cloned.1.call-start
  88.7 7.0 %all-to-all-done = bf16[2,32,32]{2,0,1:T(2,128)(2,1)S(1)} async-done(((bf16[2,32,32]{2,0,1:T(2,128)(2,1)}), bf16[2,32,32]{2,0,1:T(2,128)(2,1)S(1)}, u32[]{:S(2)}, u32[]{:S(2)}) %all-to-all-start) | async-done | bytes 4128 | tf_op jit(solution)/shard_map/all_to_all | solution.py:115
  95.8 0.0 copy-done.5
  95.8 0.2 fusion.52
  96.0 0.0 copy-done.4
  96.0 0.1 multiply_add_fusion.1
  96.1 0.4 dynamic_update_slice.3
  96.5 0.0 copy-start.2
  96.5 0.8 copy-done.2
  97.3 0.0 all-reduce.9.cloned.1.call-update
  97.3 0.0 all-reduce.11.cloned.1.call-start
  97.4 0.0 copy-done.7
  97.4 0.0 copy-done.8
  97.4 127.8 %all-reduce.9.cloned.1.call-done = f32[64,2048]{1,0:T(8,128)} async-done(((f32[64,2048]{1,0:T(8,128)}), f32[64,2048]{1,0:T(8,128)}) %all-reduce.9.cloned.1.call-update) | async-done | bytes 524304 | tf_op jit(solution)/shard_map/psum | solution.py:119
  225.2 1.2 fusion.44
  226.4 1.2 multiply_convert_fusion
  227.6 0.2 fusion.6
  227.8 0.0 copy-done.6
  227.8 0.2 fusion.53
  228.0 0.0 copy-done.9
  228.1 1.5 fusion.55
  229.6 2.1 fusion.54
  231.7 0.0 copy-done
  231.7 2.5 fusion.1
  234.2 0.0 copy-start.11
  234.2 0.0 copy-start.1
  234.2 3.2 convolution_add_fusion
  237.4 0.0 all-reduce.11.cloned.1.call-update
  237.5 0.0 copy-done.11
  237.5 128.2 %all-reduce.11.cloned.1.call-done = f32[64,2048]{1,0:T(8,128)} async-done(((f32[64,2048]{1,0:T(8,128)}), f32[64,2048]{1,0:T(8,128)}) %all-reduce.11.cloned.1.call-update) | async-done | bytes 524304 | tf_op jit(solution)/shard_map/psum | solution.py:144
  365.7 0.0 copy-done.1
  365.7 1.4 fusion.43
  367.1 0.7 fusion.28
  (19 shorter events, 0.2 us)
Async XLA Ops:
  6.5 225.2 %copy-start = (bf16[512,2048]{1,0:T(8,128)(2,1)S(1)}, bf16[512,2048]{1,0:T(8,128)(2,1)}, u32[]{:S(2)}) copy-start(bf16[512,2048]{1,0:T(8,128)(2,1)} %param.42) | copy-start | bytes 6291460
  65.0 6.2 %copy-start.3 = (f32[2,1024,16]{1,2,0:T(8,128)S(1)}, f32[2,1024,16]{1,2,0:T(8,128)}, u32[]{:S(2)}) copy-start(f32[2,1024,16]{1,2,0:T(8,128)} %param.30) | copy-start | bytes 393220
  71.4 2.9 copy-start.10
  81.0 14.8 %copy-start.5 = (bf16[32,2048]{1,0:T(8,128)(2,1)S(1)}, bf16[32,2048]{1,0:T(8,128)(2,1)}, u32[]{:S(2)}) copy-start(bf16[32,2048]{1,0:T(8,128)(2,1)} %param.32) | copy-start | bytes 393220
  81.0 15.0 %copy-start.4 = (bf16[64,64]{1,0:T(8,128)(2,1)S(1)}, bf16[64,64]{1,0:T(8,128)(2,1)}, u32[]{:S(2)}) copy-start(bf16[64,64]{1,0:T(8,128)(2,1)} %param.22) | copy-start | bytes 24580
  81.0 16.4 %copy-start.7 = (bf16[2048]{0:T(1024)(128)(2,1)S(1)}, bf16[2048]{0:T(1024)(128)(2,1)}, u32[]{:S(2)}) copy-start(bf16[2048]{0:T(1024)(128)(2,1)} %param.33) | copy-start | bytes 12292
  81.0 16.4 %copy-start.8 = (bf16[2048]{0:T(1024)(128)(2,1)S(1)}, bf16[2048]{0:T(1024)(128)(2,1)}, u32[]{:S(2)}) copy-start(bf16[2048]{0:T(1024)(128)(2,1)} %param.36) | copy-start | bytes 12292
  84.4 143.4 %copy-start.6 = (bf16[2048,4]{0,1:T(4,128)(2,1)S(1)}, bf16[2048,4]{0,1:T(4,128)(2,1)}, u32[]{:S(2)}) copy-start(bf16[2048,4]{0,1:T(4,128)(2,1)} %param.34) | copy-start | bytes 49156
  84.4 143.6 %copy-start.9 = (s32[64,2]{0,1:T(2,128)S(1)}, s32[64,2]{0,1:T(2,128)}, u32[]{:S(2)}) copy-start(s32[64,2]{0,1:T(2,128)} %param.35) | copy-start | bytes 1540
  85.2 10.5 %all-to-all-start = ((bf16[2,32,32]{2,0,1:T(2,128)(2,1)}), bf16[2,32,32]{2,0,1:T(2,128)(2,1)S(1)}, u32[]{:S(2)}, u32[]{:S(2)}) async-start(bf16[2,32,32]{2,0,1:T(2,128)(2,1)} %copy.41), calls=%async_computation | async-start | bytes 32768 | tf_op jit(solution)/shard_map/all_to_all | solution.py:115
  88.6 136.6 %all-reduce.9.cloned.1.call-start = ((), (), s32[]{:S(2)}) async-start(), calls=%async_computation.1 | async-start | bytes 1048576 | tf_op jit(solution)/shard_map/psum | solution.py:119
  96.5 0.8 copy-start.2
  97.3 268.4 %all-reduce.11.cloned.1.call-start = ((), (), s32[]{:S(2)}) async-start(), calls=%async_computation.2 | async-start | bytes 1048576 | tf_op jit(solution)/shard_map/psum | solution.py:144
  234.2 3.3 copy-start.11
  234.2 131.5 %copy-start.1 = (f32[64,2048]{1,0:T(8,128)S(1)}, f32[64,2048]{1,0:T(8,128)}, u32[]{:S(2)}) copy-start(f32[64,2048]{1,0:T(8,128)} %all-reduce.9.cloned.1.call-done) | copy-start | bytes 1572868
Sparse Core Ops, SparseCore 0:
  97.4 127.7 all-reduce.8
  237.6 128.0 all-reduce.10
where the time goes:
time: 375 us
  waiting for transfers between devices  263 us (70%)
  blocking collectives  52.3 us (14%)
  matrix products  20.2 us (5%)
  local copies, waits for them, and re-layouts  14.8 us (4%)
  between operations  13.7 us (4%)
  other arithmetic  7.07 us (2%)
    psum x1, waiting for transfers between devices, shards(): branch = lax.psum(local_branch, 'ep')  128 us
    psum x1, waiting for transfers between devices, shards(): lax.psum(lax.dynamic_update_slice_in_dim(partial_sum, placed, offset, 1),...  128 us
    unnamed x1, blocking collectives  52.3 us
    unnamed x27, local copies, waits for them, and re-layouts  13.3 us
  transfers between devices with their start and end apart: 3, of which 3 were waited for; matrix products, arithmetic and copies ran while one was open for 0% of the time, Pallas kernels for 0%

commit v1 on v0

--- a/solution.py
+++ b/solution.py
@@ -141,7 +141,9 @@
     local_branch = jnp.dot(
         expert_hidden, expert_w_down, preferred_element_type=jnp.float32
     ) + jnp.dot(dense_hidden, dense_w_down, preferred_element_type=jnp.float32)
-    branch = lax.psum(local_branch, "ep")
+    branch = local_branch
+    for hop in (1, 2, 4, 8, 16):
+        branch = branch + lax.ppermute(branch, "ep", [(dev, dev ^ hop) for dev in range(32)])
     final = residual_scale * normed.astype(jnp.float32) + branch
     center = jnp.mean(final, axis=-1, keepdims=True)
     second = jnp.mean(final * final, axis=-1, keepdims=True)

time: 375 us -> 311 us (0.83)
  waiting for transfers between devices: 263 us -> 194 us
  starting transfers between devices: 3.51 us -> 9.67 us
    psum x1 -> x0, waiting for transfers between devices: 128 us -> none  [shards(): branch = lax.psum(local_branch, 'ep')]
    ppermute x0 -> x5, waiting for transfers between devices: none -> 58.9 us  [shards(): lax.ppermute(branch, 'ep', [(dev, dev ^ hop) for dev in range(32)])]
    ppermute x0 -> x5, starting transfers between devices: none -> 6.2 us  [shards(): lax.ppermute(branch, 'ep', [(dev, dev ^ hop) for dev in range(32)])]
  transfers between devices with their start and end apart: 3 -> 7, of which waited for: 3 -> 7; matrix products, arithmetic and copies ran while one was open for 0% -> 0% of each run, Pallas kernels for 0% -> 0%
where the time goes in v1:
time: 311 us; the launch traced here: 310 us
  waiting for transfers between devices  194 us (62%)
  blocking collectives  52.3 us (17%)
  matrix products  19.4 us (6%)
  local copies, waits for them, and re-layouts  14.8 us (5%)
  between operations  13.7 us (4%)
  starting transfers between devices  9.67 us (3%)
  other arithmetic  6.29 us (2%)
    psum x1, waiting for transfers between devices, shards(): lax.psum(lax.dynamic_update_slice_in_dim(partial_sum, placed, offset, 1),...  128 us
    ppermute x5, waiting for transfers between devices, shards(): lax.ppermute(branch, 'ep', [(dev, dev ^ hop) for dev in range(32)])  58.9 us
    unnamed x1, blocking collectives  52.3 us
    unnamed x27, local copies, waits for them, and re-layouts  13.3 us
    all_to_all x1, waiting for transfers between devices, shards(): lax.all_to_all(attn, 'ep', split_axis=1, concat_axis=0, tiled=True)  7.05 us
  transfers between devices with their start and end apart: 7, of which 7 were waited for; matrix products, arithmetic and copies ran while one was open for 0% of the time, Pallas kernels for 0%

profile of v1, /device:TPU:0, one launch (start us, length us, event | category | flops | bytes accessed | tf_op | source)
XLA Modules:
  0.0 309.8 jit_solution(988514097004039675)
XLA Ops:
  6.5 0.0 copy-start
  6.5 0.8 broadcast_add_fusion
  7.3 0.7 iota_compare_fusion
  8.1 0.8 fusion.49
  8.9 1.1 fusion.47
  10.0 1.1 fusion.50
  11.1 1.1 fusion.51
  12.2 52.3 %all-reduce.9 = (bf16[64,1024]{1,0:T(8,128)(2,1)S(1)}, f32[64,16]{1,0:T(8,128)S(1)}, bf16[64,1024]{1,0:T(8,128)(2,1)S(1)}, bf16[64,1024]{1,0:T(8,128)(2,1)S(1)}) all-reduce(f32[64,1024]{1,0:T(8,128)S(1)} %fusion.47, f32[64,16]{1,0:T(8,128)S(1)} %fusion.49, f32[64,1024]{1,0:T(8,128)S(1)} %fusion.50, ...), channel_id=2, replica_groups=mesh['grp'=1,'ep'=32] {'ep'}, use_global_device_ids=true, to_apply=%region_0.0.clone | all-reduce | flops 197632 | bytes 1187840
  64.5 0.1 reshape.129
  64.6 0.1 reshape.141
  64.7 0.1 compare_convert_fusion
  64.8 0.1 reshape.133
  64.9 0.1 reshape.132
  64.9 6.2 %copy.39 = bf16[2,1024,1024]{1,2,0:T(8,128)(2,1)} copy(bf16[2,1024,1024]{2,1,0:T(8,128)(2,1)} %param.28) | data formatting | bytes 8388608 | tf_op args[6]
  71.2 0.1 multiply_reduce_fusion.2
  71.3 0.1 multiply_reduce_fusion.3
  71.4 2.9 fusion.48
  74.3 0.2 fusion.45
  74.5 0.2 fusion.16
  74.6 0.1 fusion.25
  74.8 6.2 %copy.40 = bf16[2,1024,1024]{1,2,0:T(8,128)(2,1)} copy(bf16[2,1024,1024]{2,1,0:T(8,128)(2,1)} %param.29) | data formatting | bytes 8388608 | tf_op args[7]
  81.0 3.4 %fusion.8 = f32[2,16,1,64]{3,2,1,0:T(1,128)S(1)} fusion(bf16[2,1024,16,64]{1,3,2,0:T(8,128)(2,1)} %bitcast.57, bf16[2,16,1024,1]{2,1,0,3:T(8,128)(2,1)S(1)} %fusion.25), kind=kOutput, calls=%fused_computation.18 | convolution fusion | flops 4194304 | bytes 4268032 | tf_op jit(solution)/shard_map/shl,slhd->shd/dot_general | solution.py:60
  84.4 0.1 add_convert_fusion
  84.5 0.1 all_to_all.14
  84.6 0.6 copy.41
  85.2 3.4 %all-to-all-start = ((bf16[2,32,32]{2,0,1:T(2,128)(2,1)}), bf16[2,32,32]{2,0,1:T(2,128)(2,1)S(1)}, u32[]{:S(2)}, u32[]{:S(2)}) async-start(bf16[2,32,32]{2,0,1:T(2,128)(2,1)} %copy.41), calls=%async_computation | async-start | bytes 32768 | tf_op jit(solution)/shard_map/all_to_all | solution.py:115
  88.6 0.0 all-reduce.8.cloned.1.call-start
  88.7 7.0 %all-to-all-done = bf16[2,32,32]{2,0,1:T(2,128)(2,1)S(1)} async-done(((bf16[2,32,32]{2,0,1:T(2,128)(2,1)}), bf16[2,32,32]{2,0,1:T(2,128)(2,1)S(1)}, u32[]{:S(2)}, u32[]{:S(2)}) %all-to-all-start) | async-done | bytes 4128 | tf_op jit(solution)/shard_map/all_to_all | solution.py:115
  95.7 0.0 copy-done.5
  95.7 0.2 fusion.52
  95.9 0.1 multiply_add_fusion
  96.0 0.4 dynamic_update_slice.3
  96.5 0.8 copy-done.2
  97.3 0.0 all-reduce.8.cloned.1.call-update
  97.3 0.0 copy-done.7
  97.4 127.8 %all-reduce.8.cloned.1.call-done = f32[64,2048]{1,0:T(8,128)} async-done(((f32[64,2048]{1,0:T(8,128)}), f32[64,2048]{1,0:T(8,128)}) %all-reduce.8.cloned.1.call-update) | async-done | bytes 524304 | tf_op jit(solution)/shard_map/psum | solution.py:119
  225.2 1.2 fusion.44
  226.4 1.2 multiply_convert_fusion
  227.6 0.2 fusion.6
  227.8 0.2 fusion.53
  228.0 0.0 copy-done.9
  228.0 1.5 fusion.55
  229.6 2.1 fusion.54
  231.7 0.0 copy-done
  231.7 2.5 fusion.1
  234.2 2.3 convolution_add_fusion
  236.5 0.1 collective-permute-start
  236.6 1.9 collective-permute-done
  238.5 0.1 add.114
  238.6 0.0 copy-start.11
  238.6 1.5 collective-permute-start.1
  240.2 12.5 %collective-permute-done.1 = f32[64,2048]{1,0:T(8,128)S(1)} collective-permute-done((f32[64,2048]{1,0:T(8,128)S(1)}, f32[64,2048]{1,0:T(8,128)S(1)}, u32[]{:S(2)}, u32[]{:S(2)}) %collective-permute-start.1) | collective-permute-done | bytes 524320 | tf_op jit(solution)/shard_map/ppermute | solution.py:146
  252.6 0.1 add.115
  252.7 1.5 collective-permute-start.2
  254.2 11.6 %collective-permute-done.2 = f32[64,2048]{1,0:T(8,128)S(1)} collective-permute-done((f32[64,2048]{1,0:T(8,128)S(1)}, f32[64,2048]{1,0:T(8,128)S(1)}, u32[]{:S(2)}, u32[]{:S(2)}) %collective-permute-start.2) | collective-permute-done | bytes 524320 | tf_op jit(solution)/shard_map/ppermute | solution.py:146
  265.9 0.1 add.116
  265.9 1.5 collective-permute-start.3
  267.5 10.8 %collective-permute-done.3 = f32[64,2048]{1,0:T(8,128)S(1)} collective-permute-done((f32[64,2048]{1,0:T(8,128)S(1)}, f32[64,2048]{1,0:T(8,128)S(1)}, u32[]{:S(2)}, u32[]{:S(2)}) %collective-permute-start.3) | collective-permute-done | bytes 524320 | tf_op jit(solution)/shard_map/ppermute | solution.py:146
  278.3 0.1 add.117
  278.3 1.5 collective-permute-start.4
  279.8 0.0 copy-done.11
  279.9 22.1 %collective-permute-done.4 = f32[64,2048]{1,0:T(8,128)S(1)} collective-permute-done((f32[64,2048]{1,0:T(8,128)S(1)}, f32[64,2048]{1,0:T(8,128)S(1)}, u32[]{:S(2)}, u32[]{:S(2)}) %collective-permute-start.4) | collective-permute-done | bytes 524320 | tf_op jit(solution)/shard_map/ppermute | solution.py:146
  301.9 0.3 fusion.43
  302.3 0.7 fusion.28
  (30 shorter events, 0.2 us)
Async XLA Ops:
  6.5 225.1 %copy-start = (bf16[512,2048]{1,0:T(8,128)(2,1)S(1)}, bf16[512,2048]{1,0:T(8,128)(2,1)}, u32[]{:S(2)}) copy-start(bf16[512,2048]{1,0:T(8,128)(2,1)} %param.42) | copy-start | bytes 6291460
  64.9 6.2 %copy-start.3 = (f32[2,1024,16]{1,2,0:T(8,128)S(1)}, f32[2,1024,16]{1,2,0:T(8,128)}, u32[]{:S(2)}) copy-start(f32[2,1024,16]{1,2,0:T(8,128)} %param.30) | copy-start | bytes 393220
  71.4 2.9 copy-start.10
  81.0 14.8 %copy-start.5 = (bf16[32,2048]{1,0:T(8,128)(2,1)S(1)}, bf16[32,2048]{1,0:T(8,128)(2,1)}, u32[]{:S(2)}) copy-start(bf16[32,2048]{1,0:T(8,128)(2,1)} %param.32) | copy-start | bytes 393220
  81.0 15.0 %copy-start.4 = (bf16[64,64]{1,0:T(8,128)(2,1)S(1)}, bf16[64,64]{1,0:T(8,128)(2,1)}, u32[]{:S(2)}) copy-start(bf16[64,64]{1,0:T(8,128)(2,1)} %param.22) | copy-start | bytes 24580
  81.0 16.3 %copy-start.7 = (bf16[2048]{0:T(1024)(128)(2,1)S(1)}, bf16[2048]{0:T(1024)(128)(2,1)}, u32[]{:S(2)}) copy-start(bf16[2048]{0:T(1024)(128)(2,1)} %param.33) | copy-start | bytes 12292
  81.0 16.4 %copy-start.8 = (bf16[2048]{0:T(1024)(128)(2,1)S(1)}, bf16[2048]{0:T(1024)(128)(2,1)}, u32[]{:S(2)}) copy-start(bf16[2048]{0:T(1024)(128)(2,1)} %param.36) | copy-start | bytes 12292
  84.4 143.4 %copy-start.6 = (bf16[2048,4]{0,1:T(4,128)(2,1)S(1)}, bf16[2048,4]{0,1:T(4,128)(2,1)}, u32[]{:S(2)}) copy-start(bf16[2048,4]{0,1:T(4,128)(2,1)} %param.34) | copy-start | bytes 49156
  84.4 143.6 %copy-start.9 = (s32[64,2]{0,1:T(2,128)S(1)}, s32[64,2]{0,1:T(2,128)}, u32[]{:S(2)}) copy-start(s32[64,2]{0,1:T(2,128)} %param.35) | copy-start | bytes 1540
  85.2 10.5 %all-to-all-start = ((bf16[2,32,32]{2,0,1:T(2,128)(2,1)}), bf16[2,32,32]{2,0,1:T(2,128)(2,1)S(1)}, u32[]{:S(2)}, u32[]{:S(2)}) async-start(bf16[2,32,32]{2,0,1:T(2,128)(2,1)} %copy.41), calls=%async_computation | async-start | bytes 32768 | tf_op jit(solution)/shard_map/all_to_all | solution.py:115
  88.6 136.6 %all-reduce.8.cloned.1.call-start = ((), (), s32[]{:S(2)}) async-start(), calls=%async_computation.1 | async-start | bytes 1048576 | tf_op jit(solution)/shard_map/psum | solution.py:119
  96.5 0.8 copy-start.2
  236.5 2.0 collective-permute-start
  238.6 41.3 %copy-start.11 = (bf16[64]{0:T(256)(128)(2,1)S(1)}, bf16[64]{0:T(256)(128)(2,1)}, u32[]{:S(2)}) copy-start(bf16[64]{0:T(256)(128)(2,1)} %param.43) | copy-start | bytes 388
  238.6 63.3 %copy-start.1 = (f32[64,2048]{1,0:T(8,128)S(1)}, f32[64,2048]{1,0:T(8,128)}, u32[]{:S(2)}) copy-start(f32[64,2048]{1,0:T(8,128)} %all-reduce.8.cloned.1.call-done) | copy-start | bytes 1572868
  238.6 14.0 %collective-permute-start.1 = (f32[64,2048]{1,0:T(8,128)S(1)}, f32[64,2048]{1,0:T(8,128)S(1)}, u32[]{:S(2)}, u32[]{:S(2)}) collective-permute-start(f32[64,2048]{1,0:T(8,128)S(1)} %add.114), channel_id=1, source_target_pairs={{0,2},{1,3},{2,0},{3,1},{4,6},{5,7},{6,4},{7,5},{8,10},{9,11},{10,... | collective-permute-start | bytes 1572872 | tf_op jit(solution)/shard_map/ppermute | solution.py:146
  252.7 13.2 %collective-permute-start.2 = (f32[64,2048]{1,0:T(8,128)S(1)}, f32[64,2048]{1,0:T(8,128)S(1)}, u32[]{:S(2)}, u32[]{:S(2)}) collective-permute-start(f32[64,2048]{1,0:T(8,128)S(1)} %add.115), channel_id=1, source_target_pairs={{0,4},{1,5},{2,6},{3,7},{4,0},{5,1},{6,2},{7,3},{8,12},{9,13},{10,... | collective-permute-start | bytes 1572872 | tf_op jit(solution)/shard_map/ppermute | solution.py:146
  265.9 12.3 %collective-permute-start.3 = (f32[64,2048]{1,0:T(8,128)S(1)}, f32[64,2048]{1,0:T(8,128)S(1)}, u32[]{:S(2)}, u32[]{:S(2)}) collective-permute-start(f32[64,2048]{1,0:T(8,128)S(1)} %add.116), channel_id=1, source_target_pairs={{0,8},{1,9},{2,10},{3,11},{4,12},{5,13},{6,14},{7,15},{8,0},{9,1},... | collective-permute-start | bytes 1572872 | tf_op jit(solution)/shard_map/ppermute | solution.py:146
  278.3 23.6 %collective-permute-start.4 = (f32[64,2048]{1,0:T(8,128)S(1)}, f32[64,2048]{1,0:T(8,128)S(1)}, u32[]{:S(2)}, u32[]{:S(2)}) collective-permute-start(f32[64,2048]{1,0:T(8,128)S(1)} %add.117), channel_id=1, source_target_pairs={{0,16},{1,17},{2,18},{3,19},{4,20},{5,21},{6,22},{7,23},{8,24},{9,... | collective-permute-start | bytes 1572872 | tf_op jit(solution)/shard_map/ppermute | solution.py:146
Sparse Core Ops, SparseCore 0:
  97.4 127.7 all-reduce.7
